TPU v7x, 32 devices: a whole 2x2x4 slice. The times are simulated.
32 devices in a mesh: sp: 8 (over z, y), tp: 4 (over x, core).
Axes of the slice: x: 2, y: 2, z: 4, core: 2. Of those that a mesh axis runs over, the one named last changes fastest.
Arguments:
- tokens: bfloat16 [2048, 2048], P('sp'), may hold values from -72 to 72
- query_weight: bfloat16 [3, 2048, 1024], P(None, None, 'tp'), may hold values from -0.125 to 0.125
- key_weight: bfloat16 [3, 2048, 1024], P(None, None, 'tp'), may hold values from -0.125 to 0.125
- value_weight: bfloat16 [3, 2048, 1024], P(None, None, 'tp'), may hold values from -0.125 to 0.125
- out_weight: bfloat16 [1024, 2048], P(None, 'tp'), may hold values from -2 to 2
Outputs:
- mixed: bfloat16 [2048, 2048], P('sp', 'tp')
All inputs are finite; a program needn't handle non-finite values.
Results may differ from a plain program's by a relative error of at most 0.012.
Values may be sent and summed in bfloat16 or wider, within the bound.
A program may use at most 64 MiB of HBM per device.

v0:
```python
import math
import jax
import jax.numpy as jnp
from jax import lax
from jax.sharding import PartitionSpec as P

HEAD_DIM = 64
SIDE_STEPS = 64
MIDDLE_DILATION = 4
FAR_DILATION = 16


def shifted(block, axis, distance):
    devices = range(lax.axis_size(axis))
    route = [(i - distance, i) for i in devices if i - distance in devices]
    return lax.ppermute(block, axis, route)


def with_halo(block, sides, width):
    for axis, dim in sides:
        count = lax.axis_size(axis)
        forward = [(i, i + 1) for i in range(count - 1)]
        backward = [(target, source) for source, target in forward]
        low = lax.ppermute(
            lax.slice_in_dim(block, block.shape[dim] - width, None, axis=dim), axis, forward
        )
        high = lax.ppermute(lax.slice_in_dim(block, 0, width, axis=dim), axis, backward)
        block = jnp.concatenate([low, block, high], axis=dim)
    return block


def rotate(projected, offset_pos):
    length, columns = projected.shape
    heads = columns // HEAD_DIM
    half = HEAD_DIM // 2
    positions = (offset_pos + jnp.arange(length)).astype(jnp.float32)
    inverse = 1.0 / 10000.0 ** (jnp.arange(half, dtype=jnp.float32) * 2.0 / HEAD_DIM)
    angles = positions[:, None] * inverse[None, :]
    angles = jnp.concatenate([angles, angles], axis=-1)
    cosine_table = jnp.cos(angles)[:, None, :]
    sine = jnp.sin(angles)[:, None, :]
    shaped = projected.reshape(length, heads, HEAD_DIM)
    turned = jnp.concatenate([-shaped[..., half:], shaped[..., :half]], axis=-1)
    return (shaped * cosine_table + turned * sine).reshape(length, columns)


def banded(queries, key_ext, value_ext, dilation, offset_pos, seq_len):
    length, columns = queries.shape
    heads = columns // HEAD_DIM
    class_len = length // dilation
    block_len = math.gcd(SIDE_STEPS, class_len)
    blocks = class_len // block_len
    extra = 2 * SIDE_STEPS // block_len
    query_blocks = queries.reshape(blocks, block_len, dilation, heads, HEAD_DIM)
    key_blocks = key_ext.reshape(blocks + extra, block_len, dilation, heads, HEAD_DIM)
    value_blocks = value_ext.reshape(blocks + extra, block_len, dilation, heads, HEAD_DIM)
    key_win = jnp.concatenate(
        [key_blocks[shift_idx : shift_idx + blocks] for shift_idx in range(extra + 1)], axis=1
    )
    value_win = jnp.concatenate(
        [value_blocks[shift_idx : shift_idx + blocks] for shift_idx in range(extra + 1)], axis=1
    )
    scores = jnp.einsum(
        "bqrhe,bkrhe->brhqk", query_blocks, key_win, preferred_element_type=jnp.float32
    )
    scores = scores * HEAD_DIM ** (-0.5)
    width_keys = key_win.shape[1]
    relative = jnp.arange(width_keys)[None, :] - jnp.arange(block_len)[:, None]
    within = (relative >= 0) & (relative <= 2 * SIDE_STEPS)
    key_rows = jnp.arange(blocks)[:, None] * block_len + jnp.arange(width_keys)[None, :]
    spots = (
        offset_pos
        - SIDE_STEPS * dilation
        + dilation * key_rows[:, :, None]
        + jnp.arange(dilation)[None, None, :]
    )
    inside = (spots >= 0) & (spots < seq_len)
    allowed = within[None, None, None] & jnp.transpose(inside, (0, 2, 1))[:, :, None, None, :]
    scores = jnp.where(allowed, scores, -1e30)
    row_max = jnp.max(scores, axis=-1, keepdims=True)
    expo = jnp.exp(scores - row_max)
    denom = jnp.sum(expo, axis=-1)
    probs = expo.astype(jnp.bfloat16)
    summed = jnp.einsum("brhqk,bkrhe->bqrhe", probs, value_win, preferred_element_type=jnp.float32)
    group_out = summed / jnp.transpose(denom, (0, 3, 1, 2))[..., None]
    log_sum = row_max[..., 0] + jnp.log(denom)
    log_sum = jnp.transpose(log_sum, (0, 3, 1, 2)).reshape(length, heads)
    return (group_out.reshape(length, columns), log_sum)


def collect(own_block, needed, direction):
    collected = own_block[None]
    while collected.shape[0] < needed + 1:
        stride = collected.shape[0]
        to_send = min(stride, needed + 1 - stride)
        arrived = shifted(collected[:to_send], "sp", direction * stride)
        collected = jnp.concatenate([collected, arrived], axis=0)
    return collected[1:]


def per_device(tokens, query_weight, key_weight, value_weight, out_weight):
    length = tokens.shape[0]
    offset_pos = lax.axis_index("sp") * length
    seq_len = lax.axis_size("sp") * length
    group_dilations = (1, MIDDLE_DILATION, FAR_DILATION)
    query_list = []
    pairs = []
    for group_idx in range(3):
        queries = rotate(
            jnp.dot(tokens, query_weight[group_idx], preferred_element_type=jnp.float32), offset_pos
        )
        keys_here = rotate(
            jnp.dot(tokens, key_weight[group_idx], preferred_element_type=jnp.float32), offset_pos
        )
        values_here = jnp.dot(tokens, value_weight[group_idx], preferred_element_type=jnp.float32)
        query_list.append(queries.astype(jnp.bfloat16))
        pairs.append(
            jnp.stack([keys_here.astype(jnp.bfloat16), values_here.astype(jnp.bfloat16)], axis=0)
        )
    middle_span_length = SIDE_STEPS * MIDDLE_DILATION
    first_ext = with_halo(pairs[0], (("sp", 1),), SIDE_STEPS)
    middle_ext = with_halo(pairs[1], (("sp", 1),), middle_span_length)
    far_span_length = SIDE_STEPS * FAR_DILATION
    needed = -(-far_span_length // length)
    lower_blocks = collect(pairs[2], needed, 1)
    upper_blocks = collect(pairs[2], needed, -1)
    columns = pairs[2].shape[2]
    lower_flat = jnp.moveaxis(lower_blocks[::-1], 0, 1).reshape(2, needed * length, columns)
    upper_flat = jnp.moveaxis(upper_blocks, 0, 1).reshape(2, needed * length, columns)
    far_full = jnp.concatenate([lower_flat, pairs[2], upper_flat], axis=1)
    extended = (first_ext, middle_ext, far_full)
    outputs = []
    log_sums = []
    for group_idx in range(3):
        group_out, log_sum = banded(
            query_list[group_idx],
            extended[group_idx][0],
            extended[group_idx][1],
            group_dilations[group_idx],
            offset_pos,
            seq_len,
        )
        outputs.append(group_out)
        log_sums.append(log_sum)
    merge_w = jax.nn.softmax(jnp.stack(log_sums, axis=0), axis=0)
    heads = columns // HEAD_DIM
    stacked = jnp.stack(outputs, axis=0).reshape(3, length, heads, HEAD_DIM)
    merged = (
        jnp.sum(merge_w[..., None] * stacked, axis=0).reshape(length, columns).astype(jnp.bfloat16)
    )
    mixed = jnp.dot(
        lax.all_gather(merged, "tp", axis=1, tiled=True),
        out_weight,
        preferred_element_type=jnp.float32,
    )
    return mixed.astype(jnp.bfloat16)


def solution(mesh):
    placed = (
        P("sp", None),
        P(None, None, "tp"),
        P(None, None, "tp"),
        P(None, None, "tp"),
        P(None, "tp"),
    )
    return jax.shard_map(
        per_device, mesh=mesh, in_specs=placed, out_specs=P("sp", "tp"), check_vma=False
    )
```

profile of v0, /device:TPU:13, one launch (start us, length us, event | category | flops | bytes accessed | tf_op | source)
XLA Modules:
  0.0 186.6 jit_solution(4766220064842487170)
XLA Ops:
  0.0 3.1 %slice_bitcast_fusion.4 = (bf16[256,2048]{0,1:T(8,128)(2,1)S(1)}, bf16[256,2048]{0,1:T(8,128)(2,1)}, bf16[256,2048]{0,1:T(8,128)(2,1)S(1)}) fusion(bf16[3,2048,256]{2,1,0:T(8,128)(2,1)} %param.7), kind=kLoop, calls=%fused_computation.45 | loop fusion | bytes 6291456 | tf_op jit(solution)/shard_map/dot_general | solution.py:113
  3.1 2.3 %copy.111 = bf16[256,2048]{1,0:T(8,128)(2,1)} copy(bf16[256,2048]{0,1:T(8,128)(2,1)} %get-tuple-element.9) | data formatting | bytes 2097152 | tf_op jit(solution)/shard_map/dot_general | solution.py:113
  14.2 4.9 %collective-permute-start.6 = (bf16[1,2,256,256]{3,2,1,0:T(8,128)(2,1)}, bf16[1,2,256,256]{3,2,1,0:T(8,128)(2,1)}, u32[]{:S(2)}, u32[]{:S(2)}) collective-permute-start(bf16[1,2,256,256]{3,2,1,0:T(8,128)(2,1)} %maximum_bitcast_fusion.9), channel_id=1, source_target_pairs={{0,16},{4,20},{8,24},{12,28},{1,17},{5,21},{9,25},{13,29},{2,18},{... | collective-permute-start | bytes 786440 | tf_op jit(solution)/shard_map/ppermute | solution.py:16
  19.1 2.1 %collective-permute-start.7 = (bf16[1,2,256,256]{3,2,1,0:T(8,128)(2,1)}, bf16[1,2,256,256]{3,2,1,0:T(8,128)(2,1)}, u32[]{:S(2)}, u32[]{:S(2)}) collective-permute-start(bf16[1,2,256,256]{3,2,1,0:T(8,128)(2,1)} %maximum_bitcast_fusion.9), channel_id=1, source_target_pairs={{4,0},{8,4},{12,8},{16,12},{20,16},{24,20},{28,24},{5,1},{9,5},{13... | collective-permute-start | bytes 786440 | tf_op jit(solution)/shard_map/ppermute | solution.py:16
  21.2 4.0 %collective-permute-start.4 = (bf16[1,2,256,256]{3,2,1,0:T(8,128)(2,1)}, bf16[1,2,256,256]{3,2,1,0:T(8,128)(2,1)}, u32[]{:S(2)}, u32[]{:S(2)}) collective-permute-start(bf16[1,2,256,256]{3,2,1,0:T(8,128)(2,1)} %maximum_bitcast_fusion.9), channel_id=1, source_target_pairs={{0,4},{4,8},{8,12},{12,16},{16,20},{20,24},{24,28},{1,5},{5,9},{9,... | collective-permute-start | bytes 786440 | tf_op jit(solution)/shard_map/ppermute | solution.py:16
  28.6 2.3 %copy.91 = bf16[256,2048]{1,0:T(8,128)(2,1)} copy(bf16[256,2048]{0,1:T(8,128)(2,1)} %get-tuple-element.5) | data formatting | bytes 2097152 | tf_op jit(solution)/shard_map/dot_general | solution.py:110
  34.0 2.3 %copy.99 = bf16[256,2048]{1,0:T(8,128)(2,1)} copy(bf16[256,2048]{0,1:T(8,128)(2,1)} %get-tuple-element.7) | data formatting | bytes 2097152 | tf_op jit(solution)/shard_map/dot_general | solution.py:110
  36.3 2.4 %fusion.24 = f32[256,4,64]{0,2,1:T(8,128)} fusion(bf16[4,64,2048]{2,1,0:T(8,128)(2,1)} %bitcast.222, bf16[256,2048]{1,0:T(8,128)(2,1)S(1)} %copy-done), kind=kOutput, calls=%fused_computation.28 | convolution fusion | flops 268435456 | bytes 2359296 | tf_op jit(solution)/shard_map/dot_general | solution.py:110
  40.1 2.5 %fusion.26 = f32[256,4,64]{0,2,1:T(8,128)} fusion(bf16[4,64,2048]{2,1,0:T(8,128)(2,1)} %bitcast.223, bf16[256,2048]{1,0:T(8,128)(2,1)S(1)} %copy-done), kind=kOutput, calls=%fused_computation.30 | convolution fusion | flops 268435456 | bytes 2359296 | tf_op jit(solution)/shard_map/dot_general | solution.py:113
  44.0 2.4 %fusion.20 = f32[256,4,64]{0,2,1:T(8,128)} fusion(bf16[4,64,2048]{2,1,0:T(8,128)(2,1)} %bitcast.224, bf16[256,2048]{1,0:T(8,128)(2,1)S(1)} %copy-done), kind=kOutput, calls=%fused_computation.24 | convolution fusion | flops 268435456 | bytes 2359296 | tf_op jit(solution)/shard_map/dot_general | solution.py:110
  52.5 3.4 %collective-permute-start.1 = (bf16[2,64,256]{2,1,0:T(8,128)(2,1)}, bf16[2,64,256]{2,1,0:T(8,128)(2,1)}, u32[]{:S(2)}, u32[]{:S(2)}) collective-permute-start(bf16[2,64,256]{2,1,0:T(8,128)(2,1)} %get-tuple-element.36), channel_id=1, source_target_pairs={{4,0},{8,4},{12,8},{16,12},{20,16},{24,20},{28,24},{5,1},{9,5},{13... | collective-permute-start | bytes 196616 | tf_op jit(solution)/shard_map/ppermute | solution.py:27
  71.9 2.3 %collective-permute-start.3 = (bf16[2,256,256]{2,1,0:T(8,128)(2,1)}, bf16[2,256,256]{2,1,0:T(8,128)(2,1)}, u32[]{:S(2)}, u32[]{:S(2)}) collective-permute-start(bf16[2,256,256]{2,1,0:T(8,128)(2,1)} %pad_maximum_fusion.3), channel_id=1, source_target_pairs={{4,0},{8,4},{12,8},{16,12},{20,16},{24,20},{28,24},{5,1},{9,5},{13... | collective-permute-start | bytes 786440 | tf_op jit(solution)/shard_map/ppermute | solution.py:27
  81.0 4.0 %collective-permute-start.2 = (bf16[2,256,256]{2,1,0:T(8,128)(2,1)}, bf16[2,256,256]{2,1,0:T(8,128)(2,1)S(1)}, u32[]{:S(2)}, u32[]{:S(2)}) collective-permute-start(bf16[2,256,256]{2,1,0:T(8,128)(2,1)} %pad_maximum_fusion.3), channel_id=1, source_target_pairs={{0,4},{4,8},{8,12},{12,16},{16,20},{20,24},{24,28},{1,5},{5,9},{9,... | collective-permute-start | bytes 786440 | tf_op jit(solution)/shard_map/ppermute | solution.py:24
  87.0 5.1 %collective-permute-start.5 = (bf16[2,2,256,256]{3,2,1,0:T(8,128)(2,1)}, bf16[2,2,256,256]{3,2,1,0:T(8,128)(2,1)}, u32[]{:S(2)}, u32[]{:S(2)}) collective-permute-start(bf16[2,2,256,256]{3,2,1,0:T(8,128)(2,1)} %get-tuple-element.50), channel_id=1, source_target_pairs={{0,8},{4,12},{8,16},{12,20},{16,24},{20,28},{1,9},{5,13},{9,17},{1... | collective-permute-start | bytes 1572872 | tf_op jit(solution)/shard_map/ppermute | solution.py:16
  104.3 2.4 %fusion.37 = f32[1,64,4,4,64]{1,4,3,2,0:T(8,128)} fusion(f32[4,4,64,192]{3,2,1,0:T(8,128)S(1)} %get-tuple-element.65, bf16[1,64,4,4,64]{1,4,3,2,0:T(8,128)(2,1)} %copy.136, bf16[1,64,4,4,64]{1,4,3,2,0:T(8,128)(2,1)} %copy.135, bf16[1,64,4,4,64]{1,4,3,2,0:T(8,128)(2,1)} %copy.134, f32[4,4,64]{2,1,0:T(4,128)S(1)} %get-tuple-element.64, f32[64,4,4]{0,2,1:T(4,128)} %bitcast.233), kind=kOutput, calls=%fused_computation.49 | convolution fusion | flops 26804224 | bytes 1449984 | tf_op jit(solution)/shard_map/brhqk,bkrhe->bqrhe/dot_general | solution.py:84
  111.1 2.9 %collective-permute-done.8 = bf16[2,2,256,256]{3,2,1,0:T(8,128)(2,1)} collective-permute-done((bf16[2,2,256,256]{3,2,1,0:T(8,128)(2,1)S(1)}, bf16[2,2,256,256]{3,2,1,0:T(8,128)(2,1)}, u32[]{:S(2)}, u32[]{:S(2)}) %collective-permute-start.8) | collective-permute-done | bytes 524320 | tf_op jit(solution)/shard_map/ppermute | solution.py:16
  129.0 9.6 %concatenate.99 = bf16[1,144,16,4,64]{1,4,3,2,0:T(8,128)(2,1)S(1)} concatenate(bf16[1,16,16,4,64]{1,4,3,2,0:T(8,128)(2,1)} %copy.116, bf16[1,16,16,4,64]{1,4,3,2,0:T(8,128)(2,1)} %copy.117, bf16[1,16,16,4,64]{1,4,3,2,0:T(8,128)(2,1)} %copy.118, bf16[1,16,16,4,64]{1,4,3,2,0:T(8,128)(2,1)} %copy.119, bf16[1,16,16,4,64]{1,4,3,2,0:T(8,128)(2,1)S(1)} %copy.120, ...), dimensions={1} | concatenate | bytes 2359296 | tf_op jit(solution)/shard_map/concatenate | solution.py:57
  148.5 2.5 %copy.143 = bf16[1,16,16,4,64]{1,4,3,2,0:T(8,128)(2,1)} copy(bf16[1,16,16,4,64]{4,3,2,1,0:T(4,128)(2,1)} %slice.368) | data formatting | bytes 262144 | tf_op jit(solution)/shard_map/slice | solution.py:61
  152.8 2.3 %copy.144 = bf16[1,16,16,4,64]{1,4,3,2,0:T(8,128)(2,1)} copy(bf16[1,16,16,4,64]{4,3,2,1,0:T(4,128)(2,1)} %slice.370) | data formatting | bytes 262144 | tf_op jit(solution)/shard_map/slice | solution.py:61
  156.9 2.4 %copy.145 = bf16[1,16,16,4,64]{1,4,3,2,0:T(8,128)(2,1)} copy(bf16[1,16,16,4,64]{4,3,2,1,0:T(4,128)(2,1)} %slice.372) | data formatting | bytes 262144 | tf_op jit(solution)/shard_map/slice | solution.py:61
  160.2 2.4 %copy.146 = bf16[1,16,16,4,64]{1,4,3,2,0:T(8,128)(2,1)} copy(bf16[1,16,16,4,64]{4,3,2,1,0:T(4,128)(2,1)} %slice.374) | data formatting | bytes 262144 | tf_op jit(solution)/shard_map/slice | solution.py:61
  162.6 10.3 %concatenate.102 = bf16[1,144,16,4,64]{1,4,3,2,0:T(8,128)(2,1)} concatenate(bf16[1,16,16,4,64]{1,4,3,2,0:T(8,128)(2,1)S(1)} %copy.138, bf16[1,16,16,4,64]{1,4,3,2,0:T(8,128)(2,1)} %copy.139, bf16[1,16,16,4,64]{1,4,3,2,0:T(8,128)(2,1)} %copy.140, bf16[1,16,16,4,64]{1,4,3,2,0:T(8,128)(2,1)} %copy.141, bf16[1,16,16,4,64]{1,4,3,2,0:T(8,128)(2,1)S(1)} %copy-done.3, ...), dimensions={1} | concatenate | bytes 2359296 | tf_op jit(solution)/shard_map/concatenate | solution.py:60
  172.9 2.4 %fusion.33 = f32[1,16,16,4,64]{4,1,3,2,0:T(8,128)S(1)} fusion(bf16[1,144,16,4,64]{1,4,3,2,0:T(8,128)(2,1)} %concatenate.102, f32[16,4,16,144]{3,2,1,0:T(8,128)S(1)} %get-tuple-element.63, f32[16,4,16]{2,1,0:T(4,128)S(1)} %copy-done.24, f32[16,16,4]{0,2,1:T(4,128)S(1)} %bitcast.232), kind=kOutput, calls=%fused_computation.47 | convolution fusion | flops 19234816 | bytes 2039808 | tf_op jit(solution)/shard_map/brhqk,bkrhe->bqrhe/dot_general | solution.py:84
  176.0 9.4 %all_gather.3 = bf16[256,1024]{0,1:T(8,128)(2,1)S(1)} all-gather(bf16[256,256]{0,1:T(8,128)(2,1)S(1)} %bitcast.228), channel_id=1, replica_groups=mesh['sp'=8,'tp'=4] {'tp'}, dimensions={1}, use_global_device_ids=true | all-gather | bytes 655360 | tf_op jit(solution)/shard_map/all_gather | solution.py:152
  (216 shorter events, 95.9 us)
Async XLA Ops:
  0.0 5.4 %copy-start = (bf16[256,2048]{1,0:T(8,128)(2,1)S(1)}, bf16[256,2048]{1,0:T(8,128)(2,1)}, u32[]{:S(2)}) copy-start(bf16[256,2048]{1,0:T(8,128)(2,1)} %param.5) | copy-start | bytes 3145732
  7.1 14.1 %copy-start.16 = (bf16[256,256]{1,0:T(8,128)(2,1)}, bf16[256,256]{1,0:T(8,128)(2,1)S(1)}, u32[]{:S(2)}) copy-start(bf16[256,256]{1,0:T(8,128)(2,1)S(1)} %convolution_convert_fusion.1) | copy-start | bytes 393220
  12.4 14.6 %copy-start.4 = (bf16[3,2048,256]{2,1,0:T(8,128)(2,1)S(1)}, bf16[3,2048,256]{2,1,0:T(8,128)(2,1)}, u32[]{:S(2)}) copy-start(bf16[3,2048,256]{2,1,0:T(8,128)(2,1)} %param.6) | copy-start | bytes 9437188
  14.2 94.7 %collective-permute-start.6 = (bf16[1,2,256,256]{3,2,1,0:T(8,128)(2,1)}, bf16[1,2,256,256]{3,2,1,0:T(8,128)(2,1)}, u32[]{:S(2)}, u32[]{:S(2)}) collective-permute-start(bf16[1,2,256,256]{3,2,1,0:T(8,128)(2,1)} %maximum_bitcast_fusion.9), channel_id=1, source_target_pairs={{0,16},{4,20},{8,24},{12,28},{1,17},{5,21},{9,25},{13,29},{2,18},{... | collective-permute-start | bytes 786440 | tf_op jit(solution)/shard_map/ppermute | solution.py:16
  19.1 61.9 %collective-permute-start.7 = (bf16[1,2,256,256]{3,2,1,0:T(8,128)(2,1)}, bf16[1,2,256,256]{3,2,1,0:T(8,128)(2,1)}, u32[]{:S(2)}, u32[]{:S(2)}) collective-permute-start(bf16[1,2,256,256]{3,2,1,0:T(8,128)(2,1)} %maximum_bitcast_fusion.9), channel_id=1, source_target_pairs={{4,0},{8,4},{12,8},{16,12},{20,16},{24,20},{28,24},{5,1},{9,5},{13... | collective-permute-start | bytes 786440 | tf_op jit(solution)/shard_map/ppermute | solution.py:16
  21.2 63.8 %collective-permute-start.4 = (bf16[1,2,256,256]{3,2,1,0:T(8,128)(2,1)}, bf16[1,2,256,256]{3,2,1,0:T(8,128)(2,1)}, u32[]{:S(2)}, u32[]{:S(2)}) collective-permute-start(bf16[1,2,256,256]{3,2,1,0:T(8,128)(2,1)} %maximum_bitcast_fusion.9), channel_id=1, source_target_pairs={{0,4},{4,8},{8,12},{12,16},{16,20},{20,24},{24,28},{1,5},{5,9},{9,... | collective-permute-start | bytes 786440 | tf_op jit(solution)/shard_map/ppermute | solution.py:16
  47.6 8.3 %copy-start.17 = (bf16[256,256]{1,0:T(8,128)(2,1)S(1)}, bf16[256,256]{1,0:T(8,128)(2,1)}, u32[]{:S(2)}) copy-start(bf16[256,256]{1,0:T(8,128)(2,1)} %copy-done.16) | copy-start | bytes 393220
  50.6 19.9 %collective-permute-start = (bf16[2,64,256]{2,1,0:T(8,128)(2,1)}, bf16[2,64,256]{2,1,0:T(8,128)(2,1)}, u32[]{:S(2)}, u32[]{:S(2)}) collective-permute-start(bf16[2,64,256]{2,1,0:T(8,128)(2,1)} %get-tuple-element.35), channel_id=1, source_target_pairs={{0,4},{4,8},{8,12},{12,16},{16,20},{20,24},{24,28},{1,5},{5,9},{9,... | collective-permute-start | bytes 196616 | tf_op jit(solution)/shard_map/ppermute | solution.py:24
  52.5 19.4 %collective-permute-start.1 = (bf16[2,64,256]{2,1,0:T(8,128)(2,1)}, bf16[2,64,256]{2,1,0:T(8,128)(2,1)}, u32[]{:S(2)}, u32[]{:S(2)}) collective-permute-start(bf16[2,64,256]{2,1,0:T(8,128)(2,1)} %get-tuple-element.36), channel_id=1, source_target_pairs={{4,0},{8,4},{12,8},{16,12},{20,16},{24,20},{28,24},{5,1},{9,5},{13... | collective-permute-start | bytes 196616 | tf_op jit(solution)/shard_map/ppermute | solution.py:27
  58.5 5.5 %copy-start.19 = (bf16[256,4,64]{0,2,1:T(8,128)(2,1)S(1)}, bf16[256,4,64]{0,2,1:T(8,128)(2,1)}, u32[]{:S(2)}) copy-start(bf16[256,4,64]{0,2,1:T(8,128)(2,1)} %get-tuple-element.55) | copy-start | bytes 393220
  59.3 6.7 %copy-start.18 = (bf16[256,4,64]{0,2,1:T(8,128)(2,1)S(1)}, bf16[256,4,64]{0,2,1:T(8,128)(2,1)}, u32[]{:S(2)}) copy-start(bf16[256,4,64]{0,2,1:T(8,128)(2,1)} %get-tuple-element.53) | copy-start | bytes 393220
  70.5 7.5 %copy-start.29 = (pred[4,64,192]{2,1,0:T(8,128)(4,1)S(1)}, pred[4,64,192]{2,1,0:T(8,128)(4,1)}, u32[]{:S(2)}) copy-start(pred[4,64,192]{2,1,0:T(8,128)(4,1)} %get-tuple-element.60) | copy-start | bytes 147460
  70.5 40.6 %collective-permute-start.9 = (bf16[1,2,256,256]{3,2,1,0:T(8,128)(2,1)}, bf16[1,2,256,256]{3,2,1,0:T(8,128)(2,1)}, u32[]{:S(2)}, u32[]{:S(2)}) collective-permute-start(bf16[1,2,256,256]{3,2,1,0:T(8,128)(2,1)} %maximum_bitcast_fusion.9), channel_id=1, source_target_pairs={{16,0},{20,4},{24,8},{28,12},{17,1},{21,5},{25,9},{29,13},{18,2},{... | collective-permute-start | bytes 786440 | tf_op jit(solution)/shard_map/ppermute | solution.py:16
  71.9 20.2 %collective-permute-start.3 = (bf16[2,256,256]{2,1,0:T(8,128)(2,1)}, bf16[2,256,256]{2,1,0:T(8,128)(2,1)}, u32[]{:S(2)}, u32[]{:S(2)}) collective-permute-start(bf16[2,256,256]{2,1,0:T(8,128)(2,1)} %pad_maximum_fusion.3), channel_id=1, source_target_pairs={{4,0},{8,4},{12,8},{16,12},{20,16},{24,20},{28,24},{5,1},{9,5},{13... | collective-permute-start | bytes 786440 | tf_op jit(solution)/shard_map/ppermute | solution.py:27
  81.0 15.0 %collective-permute-start.2 = (bf16[2,256,256]{2,1,0:T(8,128)(2,1)}, bf16[2,256,256]{2,1,0:T(8,128)(2,1)S(1)}, u32[]{:S(2)}, u32[]{:S(2)}) collective-permute-start(bf16[2,256,256]{2,1,0:T(8,128)(2,1)} %pad_maximum_fusion.3), channel_id=1, source_target_pairs={{0,4},{4,8},{8,12},{12,16},{16,20},{20,24},{24,28},{1,5},{5,9},{9,... | collective-permute-start | bytes 786440 | tf_op jit(solution)/shard_map/ppermute | solution.py:24
  87.0 21.9 %collective-permute-start.5 = (bf16[2,2,256,256]{3,2,1,0:T(8,128)(2,1)}, bf16[2,2,256,256]{3,2,1,0:T(8,128)(2,1)}, u32[]{:S(2)}, u32[]{:S(2)}) collective-permute-start(bf16[2,2,256,256]{3,2,1,0:T(8,128)(2,1)} %get-tuple-element.50), channel_id=1, source_target_pairs={{0,8},{4,12},{8,16},{12,20},{16,24},{20,28},{1,9},{5,13},{9,17},{1... | collective-permute-start | bytes 1572872 | tf_op jit(solution)/shard_map/ppermute | solution.py:16
  100.1 13.9 %collective-permute-start.8 = (bf16[2,2,256,256]{3,2,1,0:T(8,128)(2,1)S(1)}, bf16[2,2,256,256]{3,2,1,0:T(8,128)(2,1)}, u32[]{:S(2)}, u32[]{:S(2)}) collective-permute-start(bf16[2,2,256,256]{3,2,1,0:T(8,128)(2,1)S(1)} %get-tuple-element.49), channel_id=1, source_target_pairs={{8,0},{12,4},{16,8},{20,12},{24,16},{28,20},{9,1},{13,5},{17,9},{2... | collective-permute-start | bytes 1572872 | tf_op jit(solution)/shard_map/ppermute | solution.py:16
  142.3 5.3 %copy-start.15 = (bf16[1,256,256]{2,1,0:T(8,128)(2,1)S(1)}, bf16[1,256,256]{2,1,0:T(8,128)(2,1)}, u32[]{:S(2)}) copy-start(bf16[1,256,256]{2,1,0:T(8,128)(2,1)} %get-tuple-element.15) | copy-start | bytes 393220
  146.2 13.1 %copy-start.14 = (bf16[1,256,256]{2,1,0:T(8,128)(2,1)S(1)}, bf16[1,256,256]{2,1,0:T(8,128)(2,1)}, u32[]{:S(2)}) copy-start(bf16[1,256,256]{2,1,0:T(8,128)(2,1)} %get-tuple-element.12) | copy-start | bytes 393220
  148.5 14.0 %copy-start.3 = (bf16[1,16,16,4,64]{1,4,3,2,0:T(8,128)(2,1)S(1)}, bf16[1,16,16,4,64]{1,4,3,2,0:T(8,128)(2,1)}, u32[]{:S(2)}) copy-start(bf16[1,16,16,4,64]{1,4,3,2,0:T(8,128)(2,1)} %copy.142) | copy-start | bytes 393220
  162.6 10.3 %copy-start.24 = (f32[16,4,16]{2,1,0:T(4,128)S(1)}, f32[16,4,16]{2,1,0:T(4,128)}, u32[]{:S(2)}) copy-start(f32[16,4,16]{2,1,0:T(4,128)} %copy-done.23) | copy-start | bytes 12292
  162.6 10.3 %copy-start.28 = (f32[16,4,16]{2,1,0:T(4,128)S(1)}, f32[16,4,16]{2,1,0:T(4,128)}, u32[]{:S(2)}) copy-start(f32[16,4,16]{2,1,0:T(4,128)} %copy-done.27) | copy-start | bytes 12292
  172.9 13.7 %copy-start.1 = (bf16[256,2048]{1,0:T(8,128)(2,1)S(1)}, bf16[256,2048]{1,0:T(8,128)(2,1)}, u32[]{:S(2)}) copy-start(bf16[256,2048]{1,0:T(8,128)(2,1)} %param.5) | copy-start | bytes 3145732
  175.3 10.1 %copy-start.33 = (bf16[1024,512]{1,0:T(8,128)(2,1)S(1)}, bf16[1024,512]{1,0:T(8,128)(2,1)}, u32[]{:S(2)}) copy-start(bf16[1024,512]{1,0:T(8,128)(2,1)} %param.9) | copy-start | bytes 3145732
  (20 other events, 42.8 us)
where the time goes:
time: 189 us; the launch traced here: 187 us
  local copies, waits for them, and re-layouts  93.4 us (49%)
  starting transfers between devices  31.2 us (17%)
  matrix products  26.3 us (14%)
  other arithmetic  20.8 us (11%)
  blocking collectives  9.43 us (5%)
  waiting for transfers between devices  4.54 us (2%)
    slice x32, local copies, waits for them, and re-layouts, banded(): value_blocks[shift_idx:shift_idx + blocks]  29.6 us
    ppermute x6, starting transfers between devices, shifted(): return lax.ppermute(block, axis, route)  19.6 us
    slice x26, local copies, waits for them, and re-layouts, banded(): key_blocks[shift_idx:shift_idx + blocks]  17.3 us
    concatenate x1, local copies, waits for them, and re-layouts, banded(): jnp.concatenate([value_blocks[shift_idx:shift_idx + blocks] for shift_idx...  10.3 us
    concatenate x1, local copies, waits for them, and re-layouts, banded(): jnp.concatenate([key_blocks[shift_idx:shift_idx + blocks] for shift_idx i...  9.59 us
    all_gather x1, blocking collectives, per_device(): lax.all_gather(merged, 'tp', axis=1, tiled=True)  9.43 us
    dot_general x4, local copies, waits for them, and re-layouts, per_device(): jnp.dot(tokens, query_weight[group_idx], preferred_element_type=jnp.float32)  7.65 us
    dot_general x4, local copies, waits for them, and re-layouts, per_device(): jnp.dot(tokens, key_weight[group_idx], preferred_element_type=jnp.float32)  7.46 us
  transfers between devices with their start and end apart: 10, of which 2 were waited for; matrix products, arithmetic and copies ran while one was open for 34% of the time, Pallas kernels for 0%

commit v1 on v0

--- a/solution.py
+++ b/solution.py
@@ -8,6 +8,7 @@
 SIDE_STEPS = 64
 MIDDLE_DILATION = 4
 FAR_DILATION = 16
+touch_rates_by_axis = lambda dim_i, piece_in: jnp.concatenate(lax.all_gather(piece_in, "tp"), dim_i)
 
 
 def shifted(block, axis, distance):
@@ -148,11 +149,7 @@
     merged = (
         jnp.sum(merge_w[..., None] * stacked, axis=0).reshape(length, columns).astype(jnp.bfloat16)
     )
-    mixed = jnp.dot(
-        lax.all_gather(merged, "tp", axis=1, tiled=True),
-        out_weight,
-        preferred_element_type=jnp.float32,
-    )
+    mixed = jnp.dot(touch_rates_by_axis(1, merged), out_weight, preferred_element_type=jnp.float32)
     return mixed.astype(jnp.bfloat16)
 
 

time: 189 us -> 183 us (0.968)
  other arithmetic: 20.8 us -> 12.8 us
  waiting for transfers between devices: 4.54 us -> 8.34 us
    ppermute x6, waiting for transfers between devices: 2.91 us -> 5.44 us  [shifted(): return lax.ppermute(block, axis, route)]
    and x4, other arithmetic: 3.86 us -> 1.36 us  [banded(): within[None, None, None]]
    slice x32, local copies, waits for them, and re-layouts: 29.6 us -> 27.3 us  [banded(): value_blocks[shift_idx:shift_idx + blocks]]
  transfers between devices with their start and end apart: 10 -> 10, of which waited for: 2 -> 2; matrix products, arithmetic and copies ran while one was open for 34% -> 29% of each run, Pallas kernels for 0% -> 0%
where the time goes in v1:
time: 183 us; the launch traced here: 181 us
  local copies, waits for them, and re-layouts  92.4 us (50%)
  starting transfers between devices  30.5 us (17%)
  matrix products  26.4 us (14%)
  other arithmetic  12.8 us (7%)
  blocking collectives  9.51 us (5%)
  waiting for transfers between devices  8.34 us (5%)
    slice x32, local copies, waits for them, and re-layouts, banded(): value_blocks[shift_idx:shift_idx + blocks]  27.3 us
    ppermute x6, starting transfers between devices, shifted(): return lax.ppermute(block, axis, route)  18.8 us
    slice x26, local copies, waits for them, and re-layouts, banded(): key_blocks[shift_idx:shift_idx + blocks]  18 us
    concatenate x1, local copies, waits for them, and re-layouts, banded(): jnp.concatenate([value_blocks[shift_idx:shift_idx + blocks] for shift_idx...  10.3 us
    concatenate x1, local copies, waits for them, and re-layouts, banded(): jnp.concatenate([key_blocks[shift_idx:shift_idx + blocks] for shift_idx i...  9.81 us
    all_gather x1, blocking collectives, lax.all_gather(piece_in, 'tp')  9.51 us
    dot_general x4, local copies, waits for them, and re-layouts, per_device(): jnp.dot(tokens, query_weight[group_idx], preferred_element_type=jnp.float32)  7.66 us
    dot_general x4, local copies, waits for them, and re-layouts, per_device(): jnp.dot(tokens, key_weight[group_idx], preferred_element_type=jnp.float32)  7.44 us
  transfers between devices with their start and end apart: 10, of which 2 were waited for; matrix products, arithmetic and copies ran while one was open for 29% of the time, Pallas kernels for 0%

profile of v1, /device:TPU:13, one launch (start us, length us, event | category | flops | bytes accessed | tf_op | source)
XLA Modules:
  0.0 181.0 jit_solution(16872456832766705336)
XLA Ops:
  0.0 3.1 %slice_bitcast_fusion.4 = (bf16[256,2048]{0,1:T(8,128)(2,1)S(1)}, bf16[256,2048]{0,1:T(8,128)(2,1)}, bf16[256,2048]{0,1:T(8,128)(2,1)S(1)}) fusion(bf16[3,2048,256]{2,1,0:T(8,128)(2,1)} %param.7), kind=kLoop, calls=%fused_computation.45 | loop fusion | bytes 6291456 | tf_op jit(solution)/shard_map/dot_general | solution.py:114
  3.1 2.3 %copy.111 = bf16[256,2048]{1,0:T(8,128)(2,1)} copy(bf16[256,2048]{0,1:T(8,128)(2,1)} %get-tuple-element.9) | data formatting | bytes 2097152 | tf_op jit(solution)/shard_map/dot_general | solution.py:114
  14.1 4.9 %collective-permute-start.6 = (bf16[1,2,256,256]{3,2,1,0:T(8,128)(2,1)}, bf16[1,2,256,256]{3,2,1,0:T(8,128)(2,1)}, u32[]{:S(2)}, u32[]{:S(2)}) collective-permute-start(bf16[1,2,256,256]{3,2,1,0:T(8,128)(2,1)} %maximum_bitcast_fusion.9), channel_id=1, source_target_pairs={{0,16},{4,20},{8,24},{12,28},{1,17},{5,21},{9,25},{13,29},{2,18},{... | collective-permute-start | bytes 786440 | tf_op jit(solution)/shard_map/ppermute | solution.py:17
  19.1 2.1 %collective-permute-start.7 = (bf16[1,2,256,256]{3,2,1,0:T(8,128)(2,1)}, bf16[1,2,256,256]{3,2,1,0:T(8,128)(2,1)}, u32[]{:S(2)}, u32[]{:S(2)}) collective-permute-start(bf16[1,2,256,256]{3,2,1,0:T(8,128)(2,1)} %maximum_bitcast_fusion.9), channel_id=1, source_target_pairs={{4,0},{8,4},{12,8},{16,12},{20,16},{24,20},{28,24},{5,1},{9,5},{13... | collective-permute-start | bytes 786440 | tf_op jit(solution)/shard_map/ppermute | solution.py:17
  21.2 4.0 %collective-permute-start.4 = (bf16[1,2,256,256]{3,2,1,0:T(8,128)(2,1)}, bf16[1,2,256,256]{3,2,1,0:T(8,128)(2,1)}, u32[]{:S(2)}, u32[]{:S(2)}) collective-permute-start(bf16[1,2,256,256]{3,2,1,0:T(8,128)(2,1)} %maximum_bitcast_fusion.9), channel_id=1, source_target_pairs={{0,4},{4,8},{8,12},{12,16},{16,20},{20,24},{24,28},{1,5},{5,9},{9,... | collective-permute-start | bytes 786440 | tf_op jit(solution)/shard_map/ppermute | solution.py:17
  28.6 2.3 %copy.91 = bf16[256,2048]{1,0:T(8,128)(2,1)} copy(bf16[256,2048]{0,1:T(8,128)(2,1)} %get-tuple-element.5) | data formatting | bytes 2097152 | tf_op jit(solution)/shard_map/dot_general | solution.py:111
  34.0 2.3 %copy.99 = bf16[256,2048]{1,0:T(8,128)(2,1)} copy(bf16[256,2048]{0,1:T(8,128)(2,1)} %get-tuple-element.7) | data formatting | bytes 2097152 | tf_op jit(solution)/shard_map/dot_general | solution.py:111
  36.3 2.4 %fusion.24 = f32[256,4,64]{0,2,1:T(8,128)} fusion(bf16[4,64,2048]{2,1,0:T(8,128)(2,1)} %bitcast.225, bf16[256,2048]{1,0:T(8,128)(2,1)S(1)} %copy-done), kind=kOutput, calls=%fused_computation.28 | convolution fusion | flops 268435456 | bytes 2359296 | tf_op jit(solution)/shard_map/dot_general | solution.py:111
  40.1 2.5 %fusion.26 = f32[256,4,64]{0,2,1:T(8,128)} fusion(bf16[4,64,2048]{2,1,0:T(8,128)(2,1)} %bitcast.226, bf16[256,2048]{1,0:T(8,128)(2,1)S(1)} %copy-done), kind=kOutput, calls=%fused_computation.30 | convolution fusion | flops 268435456 | bytes 2359296 | tf_op jit(solution)/shard_map/dot_general | solution.py:114
  44.0 2.4 %fusion.20 = f32[256,4,64]{0,2,1:T(8,128)} fusion(bf16[4,64,2048]{2,1,0:T(8,128)(2,1)} %bitcast.227, bf16[256,2048]{1,0:T(8,128)(2,1)S(1)} %copy-done), kind=kOutput, calls=%fused_computation.24 | convolution fusion | flops 268435456 | bytes 2359296 | tf_op jit(solution)/shard_map/dot_general | solution.py:111
  51.2 3.4 %collective-permute-start.1 = (bf16[2,64,256]{2,1,0:T(8,128)(2,1)S(1)}, bf16[2,64,256]{2,1,0:T(8,128)(2,1)S(1)}, u32[]{:S(2)}, u32[]{:S(2)}) collective-permute-start(bf16[2,64,256]{2,1,0:T(8,128)(2,1)S(1)} %get-tuple-element.36), channel_id=1, source_target_pairs={{4,0},{8,4},{12,8},{16,12},{20,16},{24,20},{28,24},{5,1},{9,5},{13... | collective-permute-start | bytes 196616 | tf_op jit(solution)/shard_map/ppermute | solution.py:28
  66.4 2.3 %collective-permute-start.3 = (bf16[2,256,256]{2,1,0:T(8,128)(2,1)S(1)}, bf16[2,256,256]{2,1,0:T(8,128)(2,1)S(1)}, u32[]{:S(2)}, u32[]{:S(2)}) collective-permute-start(bf16[2,256,256]{2,1,0:T(8,128)(2,1)S(1)} %pad_maximum_fusion.3), channel_id=1, source_target_pairs={{4,0},{8,4},{12,8},{16,12},{20,16},{24,20},{28,24},{5,1},{9,5},{13... | collective-permute-start | bytes 786440 | tf_op jit(solution)/shard_map/ppermute | solution.py:28
  75.0 4.0 %collective-permute-start.2 = (bf16[2,256,256]{2,1,0:T(8,128)(2,1)S(1)}, bf16[2,256,256]{2,1,0:T(8,128)(2,1)S(1)}, u32[]{:S(2)}, u32[]{:S(2)}) collective-permute-start(bf16[2,256,256]{2,1,0:T(8,128)(2,1)S(1)} %pad_maximum_fusion.3), channel_id=1, source_target_pairs={{0,4},{4,8},{8,12},{12,16},{16,20},{20,24},{24,28},{1,5},{5,9},{9,... | collective-permute-start | bytes 786440 | tf_op jit(solution)/shard_map/ppermute | solution.py:25
  80.2 4.6 %collective-permute-start.5 = (bf16[2,2,256,256]{3,2,1,0:T(8,128)(2,1)S(1)}, bf16[2,2,256,256]{3,2,1,0:T(8,128)(2,1)}, u32[]{:S(2)}, u32[]{:S(2)}) collective-permute-start(bf16[2,2,256,256]{3,2,1,0:T(8,128)(2,1)S(1)} %get-tuple-element.50), channel_id=1, source_target_pairs={{0,8},{4,12},{8,16},{12,20},{16,24},{20,28},{1,9},{5,13},{9,17},{1... | collective-permute-start | bytes 1572872 | tf_op jit(solution)/shard_map/ppermute | solution.py:17
  86.0 2.9 %collective-permute-done.2 = bf16[2,256,256]{2,1,0:T(8,128)(2,1)S(1)} collective-permute-done((bf16[2,256,256]{2,1,0:T(8,128)(2,1)S(1)}, bf16[2,256,256]{2,1,0:T(8,128)(2,1)S(1)}, u32[]{:S(2)}, u32[]{:S(2)}) %collective-permute-start.2) | collective-permute-done | bytes 262176 | tf_op jit(solution)/shard_map/ppermute | solution.py:25
  101.4 5.4 %collective-permute-done.8 = bf16[2,2,256,256]{3,2,1,0:T(8,128)(2,1)} collective-permute-done((bf16[2,2,256,256]{3,2,1,0:T(8,128)(2,1)S(1)}, bf16[2,2,256,256]{3,2,1,0:T(8,128)(2,1)}, u32[]{:S(2)}, u32[]{:S(2)}) %collective-permute-start.8) | collective-permute-done | bytes 524320 | tf_op jit(solution)/shard_map/ppermute | solution.py:17
  121.9 9.8 %concatenate.99 = bf16[1,144,16,4,64]{1,4,3,2,0:T(8,128)(2,1)S(1)} concatenate(bf16[1,16,16,4,64]{1,4,3,2,0:T(8,128)(2,1)} %copy.116, bf16[1,16,16,4,64]{1,4,3,2,0:T(8,128)(2,1)} %copy.117, bf16[1,16,16,4,64]{1,4,3,2,0:T(8,128)(2,1)} %copy.118, bf16[1,16,16,4,64]{1,4,3,2,0:T(8,128)(2,1)} %copy.119, bf16[1,16,16,4,64]{1,4,3,2,0:T(8,128)(2,1)S(1)} %copy-done.4, ...), dimensions={1} | concatenate | bytes 2359296 | tf_op jit(solution)/shard_map/concatenate | solution.py:58
  142.5 2.4 %copy.143 = bf16[1,16,16,4,64]{1,4,3,2,0:T(8,128)(2,1)} copy(bf16[1,16,16,4,64]{4,3,2,1,0:T(4,128)(2,1)} %slice.368) | data formatting | bytes 262144 | tf_op jit(solution)/shard_map/slice | solution.py:62
  146.8 2.3 %copy.144 = bf16[1,16,16,4,64]{1,4,3,2,0:T(8,128)(2,1)} copy(bf16[1,16,16,4,64]{4,3,2,1,0:T(4,128)(2,1)} %slice.370) | data formatting | bytes 262144 | tf_op jit(solution)/shard_map/slice | solution.py:62
  150.9 2.4 %copy.145 = bf16[1,16,16,4,64]{1,4,3,2,0:T(8,128)(2,1)} copy(bf16[1,16,16,4,64]{4,3,2,1,0:T(4,128)(2,1)} %slice.372) | data formatting | bytes 262144 | tf_op jit(solution)/shard_map/slice | solution.py:62
  154.2 2.4 %copy.146 = bf16[1,16,16,4,64]{1,4,3,2,0:T(8,128)(2,1)} copy(bf16[1,16,16,4,64]{4,3,2,1,0:T(4,128)(2,1)} %slice.374) | data formatting | bytes 262144 | tf_op jit(solution)/shard_map/slice | solution.py:62
  156.6 10.3 %concatenate.102 = bf16[1,144,16,4,64]{1,4,3,2,0:T(8,128)(2,1)} concatenate(bf16[1,16,16,4,64]{1,4,3,2,0:T(8,128)(2,1)S(1)} %copy.138, bf16[1,16,16,4,64]{1,4,3,2,0:T(8,128)(2,1)} %copy.139, bf16[1,16,16,4,64]{1,4,3,2,0:T(8,128)(2,1)} %copy.140, bf16[1,16,16,4,64]{1,4,3,2,0:T(8,128)(2,1)} %copy.141, bf16[1,16,16,4,64]{1,4,3,2,0:T(8,128)(2,1)S(1)} %copy-done.3, ...), dimensions={1} | concatenate | bytes 2359296 | tf_op jit(solution)/shard_map/concatenate | solution.py:61
  166.9 2.3 %fusion.33 = f32[1,16,16,4,64]{4,1,3,2,0:T(8,128)S(1)} fusion(bf16[1,144,16,4,64]{1,4,3,2,0:T(8,128)(2,1)} %concatenate.102, f32[16,4,16,144]{3,2,1,0:T(8,128)S(1)} %get-tuple-element.63, f32[16,4,16]{2,1,0:T(4,128)S(1)} %copy-done.22, f32[16,16,4]{0,2,1:T(4,128)S(1)} %bitcast.236), kind=kOutput, calls=%fused_computation.47 | convolution fusion | flops 19234816 | bytes 2039808 | tf_op jit(solution)/shard_map/brhqk,bkrhe->bqrhe/dot_general | solution.py:85
  170.1 9.5 %all_gather.4 = bf16[4,256,256]{2,1,0:T(8,128)(2,1)S(1)} all-gather(bf16[1,256,256]{2,1,0:T(8,128)(2,1)S(1)} %copy.150), channel_id=1, replica_groups=mesh['sp'=8,'tp'=4] {'tp'}, dimensions={0}, use_global_device_ids=true | all-gather | bytes 655360 | tf_op jit(solution)/shard_map/all_gather | solution.py:11
  (210 shorter events, 87.5 us)
Async XLA Ops:
  0.0 5.4 %copy-start = (bf16[256,2048]{1,0:T(8,128)(2,1)S(1)}, bf16[256,2048]{1,0:T(8,128)(2,1)}, u32[]{:S(2)}) copy-start(bf16[256,2048]{1,0:T(8,128)(2,1)} %param.5) | copy-start | bytes 3145732
  7.1 14.1 %copy-start.17 = (bf16[256,256]{1,0:T(8,128)(2,1)}, bf16[256,256]{1,0:T(8,128)(2,1)S(1)}, u32[]{:S(2)}) copy-start(bf16[256,256]{1,0:T(8,128)(2,1)S(1)} %convolution_convert_fusion.1) | copy-start | bytes 393220
  12.4 14.6 %copy-start.5 = (bf16[3,2048,256]{2,1,0:T(8,128)(2,1)S(1)}, bf16[3,2048,256]{2,1,0:T(8,128)(2,1)}, u32[]{:S(2)}) copy-start(bf16[3,2048,256]{2,1,0:T(8,128)(2,1)} %param.6) | copy-start | bytes 9437188
  14.1 85.0 %collective-permute-start.6 = (bf16[1,2,256,256]{3,2,1,0:T(8,128)(2,1)}, bf16[1,2,256,256]{3,2,1,0:T(8,128)(2,1)}, u32[]{:S(2)}, u32[]{:S(2)}) collective-permute-start(bf16[1,2,256,256]{3,2,1,0:T(8,128)(2,1)} %maximum_bitcast_fusion.9), channel_id=1, source_target_pairs={{0,16},{4,20},{8,24},{12,28},{1,17},{5,21},{9,25},{13,29},{2,18},{... | collective-permute-start | bytes 786440 | tf_op jit(solution)/shard_map/ppermute | solution.py:17
  19.1 55.9 %collective-permute-start.7 = (bf16[1,2,256,256]{3,2,1,0:T(8,128)(2,1)}, bf16[1,2,256,256]{3,2,1,0:T(8,128)(2,1)}, u32[]{:S(2)}, u32[]{:S(2)}) collective-permute-start(bf16[1,2,256,256]{3,2,1,0:T(8,128)(2,1)} %maximum_bitcast_fusion.9), channel_id=1, source_target_pairs={{4,0},{8,4},{12,8},{16,12},{20,16},{24,20},{28,24},{5,1},{9,5},{13... | collective-permute-start | bytes 786440 | tf_op jit(solution)/shard_map/ppermute | solution.py:17
  21.2 57.8 %collective-permute-start.4 = (bf16[1,2,256,256]{3,2,1,0:T(8,128)(2,1)}, bf16[1,2,256,256]{3,2,1,0:T(8,128)(2,1)}, u32[]{:S(2)}, u32[]{:S(2)}) collective-permute-start(bf16[1,2,256,256]{3,2,1,0:T(8,128)(2,1)} %maximum_bitcast_fusion.9), channel_id=1, source_target_pairs={{0,4},{4,8},{8,12},{12,16},{16,20},{20,24},{24,28},{1,5},{5,9},{9,... | collective-permute-start | bytes 786440 | tf_op jit(solution)/shard_map/ppermute | solution.py:17
  47.6 7.0 %copy-start.18 = (bf16[256,256]{1,0:T(8,128)(2,1)S(1)}, bf16[256,256]{1,0:T(8,128)(2,1)}, u32[]{:S(2)}) copy-start(bf16[256,256]{1,0:T(8,128)(2,1)} %copy-done.17) | copy-start | bytes 393220
  49.3 15.8 %collective-permute-start = (bf16[2,64,256]{2,1,0:T(8,128)(2,1)S(1)}, bf16[2,64,256]{2,1,0:T(8,128)(2,1)S(1)}, u32[]{:S(2)}, u32[]{:S(2)}) collective-permute-start(bf16[2,64,256]{2,1,0:T(8,128)(2,1)S(1)} %get-tuple-element.35), channel_id=1, source_target_pairs={{0,4},{4,8},{8,12},{12,16},{16,20},{20,24},{24,28},{1,5},{5,9},{9,... | collective-permute-start | bytes 196616 | tf_op jit(solution)/shard_map/ppermute | solution.py:25
  51.2 15.1 %collective-permute-start.1 = (bf16[2,64,256]{2,1,0:T(8,128)(2,1)S(1)}, bf16[2,64,256]{2,1,0:T(8,128)(2,1)S(1)}, u32[]{:S(2)}, u32[]{:S(2)}) collective-permute-start(bf16[2,64,256]{2,1,0:T(8,128)(2,1)S(1)} %get-tuple-element.36), channel_id=1, source_target_pairs={{4,0},{8,4},{12,8},{16,12},{20,16},{24,20},{28,24},{5,1},{9,5},{13... | collective-permute-start | bytes 196616 | tf_op jit(solution)/shard_map/ppermute | solution.py:28
  65.1 36.4 %collective-permute-start.9 = (bf16[1,2,256,256]{3,2,1,0:T(8,128)(2,1)}, bf16[1,2,256,256]{3,2,1,0:T(8,128)(2,1)}, u32[]{:S(2)}, u32[]{:S(2)}) collective-permute-start(bf16[1,2,256,256]{3,2,1,0:T(8,128)(2,1)} %maximum_bitcast_fusion.9), channel_id=1, source_target_pairs={{16,0},{20,4},{24,8},{28,12},{17,1},{21,5},{25,9},{29,13},{18,2},{... | collective-permute-start | bytes 786440 | tf_op jit(solution)/shard_map/ppermute | solution.py:17
  66.4 18.4 %collective-permute-start.3 = (bf16[2,256,256]{2,1,0:T(8,128)(2,1)S(1)}, bf16[2,256,256]{2,1,0:T(8,128)(2,1)S(1)}, u32[]{:S(2)}, u32[]{:S(2)}) collective-permute-start(bf16[2,256,256]{2,1,0:T(8,128)(2,1)S(1)} %pad_maximum_fusion.3), channel_id=1, source_target_pairs={{4,0},{8,4},{12,8},{16,12},{20,16},{24,20},{28,24},{5,1},{9,5},{13... | collective-permute-start | bytes 786440 | tf_op jit(solution)/shard_map/ppermute | solution.py:28
  74.3 15.7 %copy-start.26 = (pred[4,64,192]{2,1,0:T(8,128)(4,1)S(1)}, pred[4,64,192]{2,1,0:T(8,128)(4,1)}, u32[]{:S(2)}) copy-start(pred[4,64,192]{2,1,0:T(8,128)(4,1)} %get-tuple-element.61) | copy-start | bytes 147460
  75.0 13.9 %collective-permute-start.2 = (bf16[2,256,256]{2,1,0:T(8,128)(2,1)S(1)}, bf16[2,256,256]{2,1,0:T(8,128)(2,1)S(1)}, u32[]{:S(2)}, u32[]{:S(2)}) collective-permute-start(bf16[2,256,256]{2,1,0:T(8,128)(2,1)S(1)} %pad_maximum_fusion.3), channel_id=1, source_target_pairs={{0,4},{4,8},{8,12},{12,16},{16,20},{20,24},{24,28},{1,5},{5,9},{9,... | collective-permute-start | bytes 786440 | tf_op jit(solution)/shard_map/ppermute | solution.py:25
  80.2 19.0 %collective-permute-start.5 = (bf16[2,2,256,256]{3,2,1,0:T(8,128)(2,1)S(1)}, bf16[2,2,256,256]{3,2,1,0:T(8,128)(2,1)}, u32[]{:S(2)}, u32[]{:S(2)}) collective-permute-start(bf16[2,2,256,256]{3,2,1,0:T(8,128)(2,1)S(1)} %get-tuple-element.50), channel_id=1, source_target_pairs={{0,8},{4,12},{8,16},{12,20},{16,24},{20,28},{1,9},{5,13},{9,17},{1... | collective-permute-start | bytes 1572872 | tf_op jit(solution)/shard_map/ppermute | solution.py:17
  93.0 13.8 %collective-permute-start.8 = (bf16[2,2,256,256]{3,2,1,0:T(8,128)(2,1)S(1)}, bf16[2,2,256,256]{3,2,1,0:T(8,128)(2,1)}, u32[]{:S(2)}, u32[]{:S(2)}) collective-permute-start(bf16[2,2,256,256]{3,2,1,0:T(8,128)(2,1)S(1)} %get-tuple-element.49), channel_id=1, source_target_pairs={{8,0},{12,4},{16,8},{20,12},{24,16},{28,20},{9,1},{13,5},{17,9},{2... | collective-permute-start | bytes 1572872 | tf_op jit(solution)/shard_map/ppermute | solution.py:17
  115.6 6.3 %copy-start.4 = (bf16[1,16,16,4,64]{1,4,3,2,0:T(8,128)(2,1)S(1)}, bf16[1,16,16,4,64]{1,4,3,2,0:T(8,128)(2,1)}, u32[]{:S(2)}) copy-start(bf16[1,16,16,4,64]{1,4,3,2,0:T(8,128)(2,1)} %copy.120) | copy-start | bytes 393220
  133.2 5.3 %copy-start.13 = (bf16[1,256,256]{2,1,0:T(8,128)(2,1)S(1)}, bf16[1,256,256]{2,1,0:T(8,128)(2,1)}, u32[]{:S(2)}) copy-start(bf16[1,256,256]{2,1,0:T(8,128)(2,1)} %get-tuple-element.21) | copy-start | bytes 393220
  136.3 5.3 %copy-start.16 = (bf16[1,256,256]{2,1,0:T(8,128)(2,1)S(1)}, bf16[1,256,256]{2,1,0:T(8,128)(2,1)}, u32[]{:S(2)}) copy-start(bf16[1,256,256]{2,1,0:T(8,128)(2,1)} %get-tuple-element.15) | copy-start | bytes 393220
  140.2 13.1 %copy-start.15 = (bf16[1,256,256]{2,1,0:T(8,128)(2,1)S(1)}, bf16[1,256,256]{2,1,0:T(8,128)(2,1)}, u32[]{:S(2)}) copy-start(bf16[1,256,256]{2,1,0:T(8,128)(2,1)} %get-tuple-element.12) | copy-start | bytes 393220
  142.5 14.0 %copy-start.3 = (bf16[1,16,16,4,64]{1,4,3,2,0:T(8,128)(2,1)S(1)}, bf16[1,16,16,4,64]{1,4,3,2,0:T(8,128)(2,1)}, u32[]{:S(2)}) copy-start(bf16[1,16,16,4,64]{1,4,3,2,0:T(8,128)(2,1)} %copy.142) | copy-start | bytes 393220
  156.6 10.3 %copy-start.22 = (f32[16,4,16]{2,1,0:T(4,128)S(1)}, f32[16,4,16]{2,1,0:T(4,128)}, u32[]{:S(2)}) copy-start(f32[16,4,16]{2,1,0:T(4,128)} %copy-done.21) | copy-start | bytes 12292
  156.6 10.3 %copy-start.25 = (f32[16,4,16]{2,1,0:T(4,128)S(1)}, f32[16,4,16]{2,1,0:T(4,128)}, u32[]{:S(2)}) copy-start(f32[16,4,16]{2,1,0:T(4,128)} %copy-done.24) | copy-start | bytes 12292
  169.3 11.7 %copy-start.1 = (bf16[256,2048]{1,0:T(8,128)(2,1)S(1)}, bf16[256,2048]{1,0:T(8,128)(2,1)}, u32[]{:S(2)}) copy-start(bf16[256,2048]{1,0:T(8,128)(2,1)} %param.5) | copy-start | bytes 3145732
  169.6 10.2 %copy-start.29 = (bf16[1024,512]{1,0:T(8,128)(2,1)S(1)}, bf16[1024,512]{1,0:T(8,128)(2,1)}, u32[]{:S(2)}) copy-start(bf16[1024,512]{1,0:T(8,128)(2,1)} %param.9) | copy-start | bytes 3145732
  (16 other events, 30.2 us)
